TPU v7x, 512 devices: a whole 4x8x8 slice. The times are simulated.
512 devices in a mesh: sp: 64 (over z, y), tp: 8 (over x, core).
Axes of the slice: x: 4, y: 8, z: 8, core: 2. Of those that a mesh axis runs over, the one named last changes fastest.
Arguments:
- latent: bfloat16 [65536, 2048], P('sp'), may hold values from -6 to 6
- context: bfloat16 [1024, 2048], P('sp'), may hold values from -6 to 6
- cond_lat: bfloat16 [2048], P('sp'), may hold values from -6 to 6
- cond_ctx: bfloat16 [2048], P('sp'), may hold values from -6 to 6
- mod_weight: bfloat16 [3, 2048, 2048], P(None, 'sp', 'tp'), may hold values from -0.125 to 0.125
- query_weight: bfloat16 [2048, 1024], P(None, 'tp'), may hold values from -4 to 4
- key_weight: bfloat16 [2048, 512], P(None, 'tp'), may hold values from -4 to 4
- value_weight: bfloat16 [2048, 512], P(None, 'tp'), may hold values from -0.125 to 0.125
- out_weight: bfloat16 [1024, 2048], P(None, 'tp'), may hold values from -1.5 to 1.5
- sink_logit: float32 [16], P('tp'), may hold values from 3 to 6
- context_bias: float32 [16], P('tp'), may hold values from -3.5 to -1.5
Outputs:
- mixed: bfloat16 [65536, 2048], P('sp', 'tp')
All inputs are finite; a program needn't handle non-finite values.
Results may differ from a plain program's by a relative error of at most 0.007.
The roundings to bfloat16 on the way count: a program that leaves them out, or rounds other values in their place, can miss the bound.
Values may be sent and summed in bfloat16 or wider, within the bound.
No kernel may reach another device: no remote copies, remote signals or barrier semaphores. Data moves between devices by JAX's collectives and lax.ppermute only.
A program may use at most 64 MiB of HBM per device.

v0:
```python
import jax
import jax.numpy as jnp
from jax import lax
from jax.sharding import PartitionSpec as P

HEAD_DIM = 64
WINDOW = 128
GRID_W = 64


norm_eps = 1e-05
rope_base = 10000.0


def copy_for_each(shard, axis):
    copies = jnp.broadcast_to(shard, (lax.axis_size(axis), *shard.shape))
    return lax.all_to_all(copies, axis, split_axis=0, concat_axis=0, tiled=True)


def of_everyone(shard, axis):
    everything = copy_for_each(shard, axis)
    return jnp.sum(everything, axis=0)


def joined_along(parts, dim):
    dims = list(parts.shape[1:])
    dims[dim] *= parts.shape[0]
    return jnp.moveaxis(parts, 0, dim).reshape(dims)


def gathered_copies(shard, axis, dim):
    return joined_along(copy_for_each(shard, axis), dim)


def padded(block, sides, width):
    for axis, dim in sides:
        count = lax.axis_size(axis)
        forward = [(i, i + 1) for i in range(count - 1)]
        backward = [(target, source) for source, target in forward]
        low = lax.ppermute(
            lax.slice_in_dim(block, block.shape[dim] - width, None, axis=dim), axis, forward
        )
        high = lax.ppermute(lax.slice_in_dim(block, 0, width, axis=dim), axis, backward)
        block = jnp.concatenate([low, block, high], axis=dim)
    return block


def rotary_tables(positions):
    grid_row = (positions // GRID_W).astype(jnp.float32)
    grid_col = (positions % GRID_W).astype(jnp.float32)
    freq_count = HEAD_DIM // 4
    inverse = rope_base ** (-jnp.arange(freq_count, dtype=jnp.float32) / freq_count)
    angles = jnp.concatenate([grid_row[:, None] * inverse, grid_col[:, None] * inverse], axis=-1)
    return (jnp.cos(angles), jnp.sin(angles))


def rotate(vectors, cos_table, sin_table):
    half_dim = vectors.shape[-1] // 2
    first_half = vectors[..., :half_dim]
    second_half = vectors[..., half_dim:]
    return jnp.concatenate(
        [
            first_half * cos_table - second_half * sin_table,
            first_half * sin_table + second_half * cos_table,
        ],
        axis=-1,
    )


def modulate(row_block, shift_scale):
    values_f = row_block.astype(jnp.float32)
    center = jnp.mean(values_f, -1, keepdims=True)
    spread = jnp.mean(jnp.square(values_f - center), -1, keepdims=True)
    normed = (values_f - center) * lax.rsqrt(spread + norm_eps)
    return (normed * (1.0 + shift_scale[1]) + shift_scale[0]).astype(jnp.bfloat16)


def softmax_parts(window_scores, context_scores, sinks):
    top_logit = jnp.maximum(
        jnp.maximum(jnp.max(window_scores, -1), jnp.max(context_scores, -1)), sinks[:, :, None]
    )
    window_exp = jnp.exp(window_scores - top_logit[..., None])
    context_exp = jnp.exp(context_scores - top_logit[..., None])
    denominator = (
        jnp.sum(window_exp, -1) + jnp.sum(context_exp, -1) + jnp.exp(sinks[:, :, None] - top_logit)
    )
    return (
        (window_exp / denominator[..., None]).astype(jnp.bfloat16),
        (context_exp / denominator[..., None]).astype(jnp.bfloat16),
    )


def attend_block(
    block_queries, block_keys, block_values, context_keys, context_values, valid, sinks, biases
):
    scale = HEAD_DIM ** (-0.5)
    window_scores = (
        jnp.einsum("qgrd,kgd->grqk", block_queries, block_keys, preferred_element_type=jnp.float32)
        * scale
    )
    window_scores = jnp.where(valid, window_scores, -jnp.inf)
    context_scores = (
        jnp.einsum(
            "qgrd,cgd->grqc", block_queries, context_keys, preferred_element_type=jnp.float32
        )
        * scale
    )
    context_scores = context_scores + biases[:, :, None, None]
    window_weights, context_weights = softmax_parts(window_scores, context_scores, sinks)
    attended = jnp.einsum(
        "grqk,kgd->qgrd", window_weights, block_values, preferred_element_type=jnp.float32
    ) + jnp.einsum(
        "grqc,cgd->qgrd", context_weights, context_values, preferred_element_type=jnp.float32
    )
    return attended.astype(jnp.bfloat16)


def on_device(
    latent,
    context,
    cond_lat,
    cond_ctx,
    mod_weight,
    query_weight,
    key_weight,
    value_weight,
    out_weight,
    sink_logit,
    context_bias,
):
    tokens_here = latent.shape[0]
    column_count = out_weight.shape[1]
    column_index = lax.axis_index("tp")
    query_cols = query_weight.shape[1]
    key_cols = key_weight.shape[1]
    heads_kv = key_cols // HEAD_DIM
    group_size = query_cols // key_cols
    activated = jax.nn.silu(jnp.stack([cond_lat, cond_ctx]).astype(jnp.float32)).astype(
        jnp.bfloat16
    )
    partial_mod = jnp.einsum(
        "cd,rde->cre", activated, mod_weight, preferred_element_type=jnp.float32
    )
    summed_mod = of_everyone(partial_mod, "sp")
    modulation = gathered_copies(summed_mod, "tp", 2)
    kv_weight = jnp.concatenate([key_weight, value_weight], axis=1)
    context_normed = modulate(context, modulation[1])
    context_kv = gathered_copies(
        jnp.dot(context_normed, kv_weight, preferred_element_type=jnp.float32).astype(jnp.bfloat16),
        "sp",
        0,
    )
    context_count = context_kv.shape[0]
    context_keys = context_kv[:, :key_cols].reshape(context_count, heads_kv, HEAD_DIM)
    context_values = context_kv[:, key_cols:].reshape(context_count, heads_kv, HEAD_DIM)
    normed = modulate(latent, modulation[0])
    merged_weight = jnp.concatenate([query_weight, key_weight, value_weight], axis=1)
    projections = jnp.dot(normed, merged_weight, preferred_element_type=jnp.float32)
    offset = lax.axis_index("sp") * tokens_here
    seq_total = tokens_here * lax.axis_size("sp")
    positions = offset + jnp.arange(tokens_here, dtype=jnp.int32)
    cos_table, sin_table = rotary_tables(positions)
    queries = rotate(
        projections[:, :query_cols].reshape(tokens_here, heads_kv * group_size, HEAD_DIM),
        cos_table[:, None, :],
        sin_table[:, None, :],
    ).astype(jnp.bfloat16)
    queries = queries.reshape(tokens_here, heads_kv, group_size, HEAD_DIM)
    keys = rotate(
        projections[:, query_cols : query_cols + key_cols].reshape(tokens_here, heads_kv, HEAD_DIM),
        cos_table[:, None, :],
        sin_table[:, None, :],
    ).astype(jnp.bfloat16)
    values = projections[:, query_cols + key_cols :].astype(jnp.bfloat16)
    keys_values = jnp.concatenate([keys.reshape(tokens_here, key_cols), values], axis=1)
    extended = padded(keys_values, (("sp", 0),), WINDOW)
    sinks = sink_logit.reshape(heads_kv, group_size)
    biases = context_bias.reshape(heads_kv, group_size)
    block_rows = min(512, tokens_here)
    span = block_rows + 2 * WINDOW
    outputs = []
    for block_index in range(tokens_here // block_rows):
        first_row = block_index * block_rows
        block_kv = extended[first_row : first_row + span]
        block_keys = block_kv[:, :key_cols].reshape(span, heads_kv, HEAD_DIM)
        block_values = block_kv[:, key_cols:].reshape(span, heads_kv, HEAD_DIM)
        query_pos = offset + first_row + jnp.arange(block_rows, dtype=jnp.int32)
        key_pos = offset + first_row - WINDOW + jnp.arange(span, dtype=jnp.int32)
        valid = (
            (jnp.abs(query_pos[:, None] - key_pos[None, :]) <= WINDOW)
            & (key_pos >= 0)[None, :]
            & (key_pos < seq_total)[None, :]
        )
        block_out = attend_block(
            queries[first_row : first_row + block_rows],
            block_keys,
            block_values,
            context_keys,
            context_values,
            valid,
            sinks,
            biases,
        )
        outputs.append(block_out.reshape(block_rows, query_cols))
    attended = jnp.concatenate(outputs, axis=0)
    projected = jnp.dot(
        gathered_copies(attended, "tp", 1), out_weight, preferred_element_type=jnp.float32
    )
    own_columns = lax.dynamic_slice_in_dim(latent, column_index * column_count, column_count, 1)
    gate_columns = lax.dynamic_slice_in_dim(
        modulation[0, 2], column_index * column_count, column_count, 0
    )
    return (own_columns.astype(jnp.float32) + gate_columns * projected).astype(jnp.bfloat16)


def solution(mesh):
    return jax.shard_map(
        on_device,
        mesh=mesh,
        in_specs=(
            P("sp", None),
            P("sp", None),
            P("sp"),
            P("sp"),
            P(None, "sp", "tp"),
            P(None, "tp"),
            P(None, "tp"),
            P(None, "tp"),
            P(None, "tp"),
            P("tp"),
            P("tp"),
        ),
        out_specs=P("sp", "tp"),
        check_vma=False,
    )
```

profile of v0, /device:TPU:1, one launch (start us, length us, event | category | flops | bytes accessed | tf_op | source)
XLA Modules:
  0.0 119.7 jit_solution(7618649978619132912)
XLA Ops:
  1.9 17.1 %all-to-all-start = ((f32[64,2,3,256]{3,1,2,0:T(2,128)}), f32[64,2,3,256]{3,1,2,0:T(2,128)S(1)}, u32[]{:S(2)}, u32[]{:S(2)}) async-start(f32[64,2,3,256]{3,1,2,0:T(2,128)} %broadcast_in_dim.18), calls=%async_computation | async-start | bytes 786432 | tf_op jit(solution)/shard_map/all_to_all | solution.py:17
  19.1 1.1 convert_reduce_fusion.1
  20.2 1.2 fusion.54
  21.5 2.8 %convert_reduce_fusion = f32[1024]{0:T(1024)S(1)} fusion(bf16[1024,2048]{1,0:T(8,128)(2,1)} %param.11), kind=kLoop, calls=%fused_computation.1 | loop fusion | flops 4193280 | bytes 4198400 | tf_op jit(solution)/shard_map/reduce_sum | solution.py:72
  24.3 1.2 %fusion.2 = f32[1024]{0:T(1024)S(1)} fusion(bf16[1024,2048]{1,0:T(8,128)(2,1)S(1)} %copy-done.1, f32[1024]{0:T(1024)S(1)} %broadcast_multiply_fusion.2), kind=kLoop, calls=%fused_computation.4 | loop fusion | flops 8387584 | bytes 4202496 | tf_op jit(solution)/shard_map/reduce_sum | solution.py:73
  27.8 6.3 %all-to-all-done = f32[64,2,3,256]{3,1,2,0:T(2,128)S(1)} async-done(((f32[64,2,3,256]{3,1,2,0:T(2,128)}), f32[64,2,3,256]{3,1,2,0:T(2,128)S(1)}, u32[]{:S(2)}, u32[]{:S(2)}) %all-to-all-start) | async-done | bytes 393248 | tf_op jit(solution)/shard_map/all_to_all | solution.py:17
  34.9 7.5 %all-to-all-start.1 = ((f32[8,2,3,256]{3,1,2,0:T(2,128)}), f32[8,2,3,256]{3,1,2,0:T(2,128)S(1)}, u32[]{:S(2)}, u32[]{:S(2)}) async-start(f32[8,2,3,256]{3,1,2,0:T(2,128)} %broadcast_in_dim.19), calls=%async_computation.1 | async-start | bytes 98304 | tf_op jit(solution)/shard_map/all_to_all | solution.py:17
  43.5 3.7 %all-to-all-done.1 = f32[8,2,3,256]{3,1,2,0:T(2,128)S(1)} async-done(((f32[8,2,3,256]{3,1,2,0:T(2,128)}), f32[8,2,3,256]{3,1,2,0:T(2,128)S(1)}, u32[]{:S(2)}, u32[]{:S(2)}) %all-to-all-start.1) | async-done | bytes 49184 | tf_op jit(solution)/shard_map/all_to_all | solution.py:17
  47.2 4.6 %fusion.8 = f32[1024,256]{0,1:T(8,128)S(1)} fusion(bf16[1024,2048]{1,0:T(8,128)(2,1)} %param.11, f32[2048]{0:T(1024)S(1)} %bitcast.191, f32[2048]{0:T(1024)S(1)} %bitcast.190, f32[1024]{0:T(1024)S(1)} %add_rsqrt_fusion, f32[1024]{0:T(1024)S(1)} %broadcast_multiply_fusion.2, bf16[2048,64]{1,0:T(8,128)(2,1)S(1)} %copy.32, bf16[2048,64]{1,0:T(8,128)(2,1)S(1)} %copy.31, ...), kind=kOutput, calls=%fused_computation.18 | convolution fusion | flops 1089470464 | bytes 6316032 | tf_op jit(solution)/shard_map/dot_general | solution.py:158
  53.0 4.6 %all-to-all-start.2 = ((bf16[64,16,128]{2,1,0:T(8,128)(2,1)}), bf16[64,16,128]{2,1,0:T(8,128)(2,1)S(1)}, u32[]{:S(2)}, u32[]{:S(2)}) async-start(bf16[64,16,128]{2,1,0:T(8,128)(2,1)} %broadcast_in_dim.22), calls=%async_computation.2 | async-start | bytes 524288 | tf_op jit(solution)/shard_map/all_to_all | solution.py:17
  58.2 2.8 %collective-permute-start = (bf16[128,128]{0,1:T(8,128)(2,1)S(1)}, bf16[128,128]{0,1:T(8,128)(2,1)S(1)}, u32[]{:S(2)}, u32[]{:S(2)}) collective-permute-start(bf16[128,128]{0,1:T(8,128)(2,1)S(1)} %get-tuple-element.11), channel_id=1, source_target_pairs={{0,8},{8,16},{16,24},{24,32},{32,40},{40,48},{48,56},{56,64},{64,7... | collective-permute-start | bytes 98312 | tf_op jit(solution)/shard_map/ppermute | solution.py:40
  61.0 1.5 %collective-permute-start.1 = (bf16[128,128]{0,1:T(8,128)(2,1)S(1)}, bf16[128,128]{0,1:T(8,128)(2,1)S(1)}, u32[]{:S(2)}, u32[]{:S(2)}) collective-permute-start(bf16[128,128]{0,1:T(8,128)(2,1)S(1)} %get-tuple-element.12), channel_id=1, source_target_pairs={{8,0},{16,8},{24,16},{32,24},{40,32},{48,40},{56,48},{64,56},{72,6... | collective-permute-start | bytes 98312 | tf_op jit(solution)/shard_map/ppermute | solution.py:43
  62.6 3.4 %collective-permute-done.1 = bf16[128,128]{0,1:T(8,128)(2,1)S(1)} collective-permute-done((bf16[128,128]{0,1:T(8,128)(2,1)S(1)}, bf16[128,128]{0,1:T(8,128)(2,1)S(1)}, u32[]{:S(2)}, u32[]{:S(2)}) %collective-permute-start.1) | collective-permute-done | bytes 32800 | tf_op jit(solution)/shard_map/ppermute | solution.py:43
  66.0 2.5 %fusion.15 = (f32[2,512]{1,0:T(2,128)S(1)}, f32[768,512,2]{1,0,2:T(8,128)}) fusion(pred[512,768]{0,1:T(8,128)(4,1)S(1)} %fusion.27, bf16[1024,2,32]{0,2,1:T(8,128)(2,1)S(1)} %get-tuple-element.8, bf16[1024,2,32]{0,2,1:T(8,128)(2,1)S(1)} %get-tuple-element.7, bf16[128,128]{0,1:T(8,128)(2,1)S(1)} %collective-permute-done.1, bf16[1024,64]{0,1:T(8,128)(2,1)S(1)} %slice.163, ...), kind=kOutput, calls=%fused_computation.30 | convolution fusion | flops 103676928 | bytes 4100096 | tf_op jit(solution)/shard_map/qgrd,kgd->grqk/dot_general | solution.py:98
  68.4 2.5 %fusion.14 = (f32[2,512]{1,0:T(2,128)S(1)}, f32[768,512,2]{1,0,2:T(8,128)}) fusion(pred[512,768]{0,1:T(8,128)(4,1)S(1)} %fusion.25, bf16[1024,2,32]{0,2,1:T(8,128)(2,1)S(1)} %get-tuple-element.7, bf16[1024,2,32]{0,2,1:T(8,128)(2,1)S(1)} %get-tuple-element.8, bf16[128,128]{0,1:T(8,128)(2,1)S(1)} %collective-permute-done, bf16[1024,64]{0,1:T(8,128)(2,1)S(1)} %slice.163, ...), kind=kOutput, calls=%fused_computation.29 | convolution fusion | flops 103676928 | bytes 4100096 | tf_op jit(solution)/shard_map/qgrd,kgd->grqk/dot_general | solution.py:98
  71.7 1.1 copy-done.3
  73.6 1.5 %fusion.10 = (f32[2,512]{1,0:T(2,128)S(1)}, f32[2,512]{1,0:T(2,128)S(1)}, f32[1024,512,2]{1,0,2:T(8,128)S(1)}) fusion(f32[1024,512,2]{1,0,2:T(8,128)S(1)} %get-tuple-element.30, f32[2,512]{1,0:T(2,128)S(1)} %maximum_maximum_fusion.1, f32[2]{0:T(128)S(1)} %copy-done.8, bf16[1024,2,32]{0,2,1:T(8,128)(2,1)S(1)} %get-tuple-element.8, ...), kind=kOutput, calls=%fused_computation.19 | convolution fusion | flops 141817856 | bytes 8925192 | tf_op jit(solution)/shard_map/qgrd,cgd->grqc/dot_general | solution.py:103
  75.1 1.2 %fusion.18 = f32[64,2,512]{2,0,1:T(8,128)S(1)} fusion(f32[1024,512,2]{1,0,2:T(8,128)S(1)} %get-tuple-element.30, f32[2,512]{1,0:T(2,128)S(1)} %get-tuple-element.23, f32[2,512]{1,0:T(2,128)S(1)} %maximum_maximum_fusion.1, f32[2]{0:T(128)S(1)} %copy-done.8, bf16[1024,128]{1,0:T(8,128)(2,1)S(1)} %bitcast.179), kind=kOutput, calls=%fused_computation.33 | convolution fusion | flops 139460608 | bytes 4726792 | tf_op jit(solution)/shard_map/grqc,cgd->qgrd/dot_general | solution.py:112
  79.1 1.2 %fusion.16 = f32[64,2,512]{2,0,1:T(8,128)S(1)} fusion(f32[1024,512,2]{1,0,2:T(8,128)S(1)} %get-tuple-element.31, f32[2,512]{1,0:T(2,128)S(1)} %exponential_add_fusion, f32[2,512]{1,0:T(2,128)S(1)} %get-tuple-element.24, f32[2]{0:T(128)S(1)} %copy-done.8, bf16[1024,128]{1,0:T(8,128)(2,1)S(1)} %bitcast.180), kind=kOutput, calls=%fused_computation.31 | convolution fusion | flops 139460608 | bytes 4726792 | tf_op jit(solution)/shard_map/grqc,cgd->qgrd/dot_general | solution.py:112
  81.4 1.1 fusion.36
  82.5 1.6 %broadcast_in_dim.26 = bf16[8,1024,128]{1,2,0:T(8,128)(2,1)} broadcast(bf16[1024,128]{0,1:T(8,128)(2,1)S(1)} %pad_maximum_fusion), dimensions={1,2} | broadcast | bytes 2359296 | tf_op jit(solution)/shard_map/broadcast_in_dim | solution.py:16
  84.2 6.7 %all-to-all-start.3 = ((bf16[8,1024,128]{1,2,0:T(8,128)(2,1)}), bf16[8,1024,128]{1,2,0:T(8,128)(2,1)S(1)}, u32[]{:S(2)}, u32[]{:S(2)}) async-start(bf16[8,1024,128]{1,2,0:T(8,128)(2,1)} %broadcast_in_dim.26), calls=%async_computation.3 | async-start | bytes 4194304 | tf_op jit(solution)/shard_map/all_to_all | solution.py:17
  90.9 26.2 %all-to-all-done.3 = bf16[8,1024,128]{1,2,0:T(8,128)(2,1)S(1)} async-done(((bf16[8,1024,128]{1,2,0:T(8,128)(2,1)}), bf16[8,1024,128]{1,2,0:T(8,128)(2,1)S(1)}, u32[]{:S(2)}, u32[]{:S(2)}) %all-to-all-start.3) | async-done | bytes 2097184 | tf_op jit(solution)/shard_map/all_to_all | solution.py:17
  117.1 2.6 %fusion.29 = bf16[1024,256]{1,0:T(8,128)(2,1)} fusion(bf16[1024,1024]{0,1:T(8,128)(2,1)S(1)} %bitcast.181, bf16[1024,256]{1,0:T(8,128)(2,1)S(1)} %copy-done, f32[256]{0:T(256)S(1)} %bitcast.192, bf16[1024,2048]{1,0:T(8,128)(2,1)} %param.11, s32[]{:T(128)S(6)} %select_n.31), kind=kOutput, calls=%fused_computation.47 | convolution fusion | flops 537919488 | bytes 3671044 | tf_op jit(solution)/shard_map/dot_general | solution.py:206
  (64 shorter events, 13.2 us)
Async XLA Ops:
  0.0 117.1 %copy-start = (bf16[1024,256]{1,0:T(8,128)(2,1)S(1)}, bf16[1024,256]{1,0:T(8,128)(2,1)}, u32[]{:S(2)}) copy-start(bf16[1024,256]{1,0:T(8,128)(2,1)} %param.19) | copy-start | bytes 1572868
  1.9 32.2 %all-to-all-start = ((f32[64,2,3,256]{3,1,2,0:T(2,128)}), f32[64,2,3,256]{3,1,2,0:T(2,128)S(1)}, u32[]{:S(2)}, u32[]{:S(2)}) async-start(f32[64,2,3,256]{3,1,2,0:T(2,128)} %broadcast_in_dim.18), calls=%async_computation | async-start | bytes 786432 | tf_op jit(solution)/shard_map/all_to_all | solution.py:17
  19.1 5.2 %copy-start.1 = (bf16[1024,2048]{1,0:T(8,128)(2,1)S(1)}, bf16[1024,2048]{1,0:T(8,128)(2,1)}, u32[]{:S(2)}) copy-start(bf16[1024,2048]{1,0:T(8,128)(2,1)} %param.11) | copy-start | bytes 12582916
  24.3 18.6 %copy-start.5 = (bf16[2048,64]{0,1:T(8,128)(2,1)S(1)}, bf16[2048,64]{0,1:T(8,128)(2,1)}, u32[]{:S(2)}) copy-start(bf16[2048,64]{0,1:T(8,128)(2,1)} %param.17) | copy-start | bytes 786436
  24.3 18.9 %copy-start.4 = (bf16[2048,64]{0,1:T(8,128)(2,1)S(1)}, bf16[2048,64]{0,1:T(8,128)(2,1)}, u32[]{:S(2)}) copy-start(bf16[2048,64]{0,1:T(8,128)(2,1)} %param.18) | copy-start | bytes 786436
  34.9 12.3 %all-to-all-start.1 = ((f32[8,2,3,256]{3,1,2,0:T(2,128)}), f32[8,2,3,256]{3,1,2,0:T(2,128)S(1)}, u32[]{:S(2)}, u32[]{:S(2)}) async-start(f32[8,2,3,256]{3,1,2,0:T(2,128)} %broadcast_in_dim.19), calls=%async_computation.1 | async-start | bytes 98304 | tf_op jit(solution)/shard_map/all_to_all | solution.py:17
  47.2 4.8 %copy-start.6 = (bf16[16,2048]{1,0:T(8,128)(2,1)S(1)}, bf16[16,2048]{1,0:T(8,128)(2,1)}, u32[]{:S(2)}) copy-start(bf16[16,2048]{1,0:T(8,128)(2,1)} %param.12) | copy-start | bytes 196612
  51.9 5.8 %copy-start.7 = (f32[1024,1,16]{0,2,1:T(8,128)S(1)}, f32[1024,1,16]{0,2,1:T(8,128)}, u32[]{:S(2)}) copy-start(f32[1024,1,16]{0,2,1:T(8,128)} %get-tuple-element.26) | copy-start | bytes 196612
  53.0 17.9 %all-to-all-start.2 = ((bf16[64,16,128]{2,1,0:T(8,128)(2,1)}), bf16[64,16,128]{2,1,0:T(8,128)(2,1)S(1)}, u32[]{:S(2)}, u32[]{:S(2)}) async-start(bf16[64,16,128]{2,1,0:T(8,128)(2,1)} %broadcast_in_dim.22), calls=%async_computation.2 | async-start | bytes 524288 | tf_op jit(solution)/shard_map/all_to_all | solution.py:17
  58.2 10.2 %collective-permute-start = (bf16[128,128]{0,1:T(8,128)(2,1)S(1)}, bf16[128,128]{0,1:T(8,128)(2,1)S(1)}, u32[]{:S(2)}, u32[]{:S(2)}) collective-permute-start(bf16[128,128]{0,1:T(8,128)(2,1)S(1)} %get-tuple-element.11), channel_id=1, source_target_pairs={{0,8},{8,16},{16,24},{24,32},{32,40},{40,48},{48,56},{56,64},{64,7... | collective-permute-start | bytes 98312 | tf_op jit(solution)/shard_map/ppermute | solution.py:40
  61.0 5.0 %collective-permute-start.1 = (bf16[128,128]{0,1:T(8,128)(2,1)S(1)}, bf16[128,128]{0,1:T(8,128)(2,1)S(1)}, u32[]{:S(2)}, u32[]{:S(2)}) collective-permute-start(bf16[128,128]{0,1:T(8,128)(2,1)S(1)} %get-tuple-element.12), channel_id=1, source_target_pairs={{8,0},{16,8},{24,16},{32,24},{40,32},{48,40},{56,48},{64,56},{72,6... | collective-permute-start | bytes 98312 | tf_op jit(solution)/shard_map/ppermute | solution.py:43
  68.4 2.5 %copy-start.8 = (f32[2]{0:T(128)S(1)}, f32[2]{0:T(128)}, u32[]{:S(2)}) copy-start(f32[2]{0:T(128)} %param.21) | copy-start | bytes 28
  70.9 0.7 copy-start.9
  70.9 1.9 %copy-start.3 = (f32[768,512,2]{1,0,2:T(8,128)S(1)}, f32[768,512,2]{1,0,2:T(8,128)}, u32[]{:S(2)}) copy-start(f32[768,512,2]{1,0,2:T(8,128)} %get-tuple-element.28) | copy-start | bytes 9437188
  76.4 1.9 %copy-start.2 = (f32[768,512,2]{1,0,2:T(8,128)S(1)}, f32[768,512,2]{1,0,2:T(8,128)}, u32[]{:S(2)}) copy-start(f32[768,512,2]{1,0,2:T(8,128)} %get-tuple-element.33) | copy-start | bytes 9437188
  84.2 32.9 %all-to-all-start.3 = ((bf16[8,1024,128]{1,2,0:T(8,128)(2,1)}), bf16[8,1024,128]{1,2,0:T(8,128)(2,1)S(1)}, u32[]{:S(2)}, u32[]{:S(2)}) async-start(bf16[8,1024,128]{1,2,0:T(8,128)(2,1)} %broadcast_in_dim.26), calls=%async_computation.3 | async-start | bytes 4194304 | tf_op jit(solution)/shard_map/all_to_all | solution.py:17
where the time goes:
time: 121 us; the launch traced here: 120 us
  starting transfers between devices  40.3 us (33%)
  waiting for transfers between devices  39.6 us (33%)
  matrix products  20.3 us (17%)
  other arithmetic  12.5 us (10%)
  local copies, waits for them, and re-layouts  6.66 us (6%)
    all_to_all x4, waiting for transfers between devices, copy_for_each(): return lax.all_to_all(copies, axis, split_axis=0, concat_axis=0, tiled=True)  36.2 us
    all_to_all x4, starting transfers between devices, copy_for_each(): return lax.all_to_all(copies, axis, split_axis=0, concat_axis=0, tiled=True)  36 us
    dot_general x2, matrix products, attend_block(): jnp.einsum('qgrd,kgd->grqk', block_queries, block_keys, preferred_element...  4.95 us
    dot_general x1, matrix products, on_device(): jnp.dot(normed, merged_weight, preferred_element_type=jnp.float32)  4.64 us
    reduce_sum x2, other arithmetic, modulate(): center = jnp.mean(values_f, -1, keepdims=True)  3.92 us
    broadcast_in_dim x4, local copies, waits for them, and re-layouts, copy_for_each(): copies = jnp.broadcast_to(shard, (lax.axis_size(axis), *shard.shape))  3.87 us
    ppermute x1, waiting for transfers between devices, padded(): lax.ppermute(lax.slice_in_dim(block, 0, width, axis=dim), axis, backward)  3.4 us
    ppermute x1, starting transfers between devices, padded(): lax.ppermute(lax.slice_in_dim(block, block.shape[dim] - width, None, axis...  2.8 us
  transfers between devices with their start and end apart: 6, of which 4 were waited for; matrix products, arithmetic and copies ran while one was open for 13% of the time, Pallas kernels for 0%

commit v1 on v0

--- a/solution.py
+++ b/solution.py
@@ -6,6 +6,7 @@
 HEAD_DIM = 64
 WINDOW = 128
 GRID_W = 64
+CORES = 2
 
 
 norm_eps = 1e-05
@@ -32,17 +33,27 @@
     return joined_along(copy_for_each(shard, axis), dim)
 
 
-def padded(block, sides, width):
-    for axis, dim in sides:
-        count = lax.axis_size(axis)
-        forward = [(i, i + 1) for i in range(count - 1)]
-        backward = [(target, source) for source, target in forward]
-        low = lax.ppermute(
-            lax.slice_in_dim(block, block.shape[dim] - width, None, axis=dim), axis, forward
-        )
-        high = lax.ppermute(lax.slice_in_dim(block, 0, width, axis=dim), axis, backward)
-        block = jnp.concatenate([low, block, high], axis=dim)
-    return block
+def neighbour_rows(rows, width, axis):
+    count = lax.axis_size(axis)
+    forward = [(i, i + 1) for i in range(count - 1)]
+    backward = [(target, source) for source, target in forward]
+    low = lax.ppermute(rows[rows.shape[0] - width :], axis, forward)
+    high = lax.ppermute(rows[:width], axis, backward)
+    return jnp.concatenate([low, high], axis=0)
+
+
+def same_core_copies(shard, axis):
+    count = lax.axis_size(axis)
+    groups = [list(range(core, count, CORES)) for core in range(CORES)]
+    copies = jnp.broadcast_to(shard, (count // CORES, *shard.shape))
+    return lax.all_to_all(
+        copies, axis, split_axis=0, concat_axis=0, tiled=True, axis_index_groups=groups
+    )
+
+
+def swapped_cores(block, axis):
+    count = lax.axis_size(axis)
+    return lax.ppermute(block, axis, [(i, i ^ 1) for i in range(count)])
 
 
 def rotary_tables(positions):
@@ -141,6 +152,7 @@
     partial_mod = jnp.einsum(
         "cd,rde->cre", activated, mod_weight, preferred_element_type=jnp.float32
     )
+    halo_rows = neighbour_rows(latent, WINDOW, "sp")
     summed_mod = of_everyone(partial_mod, "sp")
     modulation = gathered_copies(summed_mod, "tp", 2)
     kv_weight = jnp.concatenate([key_weight, value_weight], axis=1)
@@ -156,24 +168,30 @@
     normed = modulate(latent, modulation[0])
     merged_weight = jnp.concatenate([query_weight, key_weight, value_weight], axis=1)
     projections = jnp.dot(normed, merged_weight, preferred_element_type=jnp.float32)
+    halo_kv = jnp.dot(
+        modulate(halo_rows, modulation[0]), kv_weight, preferred_element_type=jnp.float32
+    )
     offset = lax.axis_index("sp") * tokens_here
     seq_total = tokens_here * lax.axis_size("sp")
-    positions = offset + jnp.arange(tokens_here, dtype=jnp.int32)
+    positions = offset - WINDOW + jnp.arange(tokens_here + 2 * WINDOW, dtype=jnp.int32)
     cos_table, sin_table = rotary_tables(positions)
+    own = slice(WINDOW, WINDOW + tokens_here)
     queries = rotate(
         projections[:, :query_cols].reshape(tokens_here, heads_kv * group_size, HEAD_DIM),
+        cos_table[own, None, :],
+        sin_table[own, None, :],
+    ).astype(jnp.bfloat16)
+    queries = queries.reshape(tokens_here, heads_kv, group_size, HEAD_DIM)
+    kv_rows = jnp.concatenate(
+        [halo_kv[:WINDOW], projections[:, query_cols:], halo_kv[WINDOW:]], axis=0
+    )
+    keys = rotate(
+        kv_rows[:, :key_cols].reshape(-1, heads_kv, HEAD_DIM),
         cos_table[:, None, :],
         sin_table[:, None, :],
     ).astype(jnp.bfloat16)
-    queries = queries.reshape(tokens_here, heads_kv, group_size, HEAD_DIM)
-    keys = rotate(
-        projections[:, query_cols : query_cols + key_cols].reshape(tokens_here, heads_kv, HEAD_DIM),
-        cos_table[:, None, :],
-        sin_table[:, None, :],
-    ).astype(jnp.bfloat16)
-    values = projections[:, query_cols + key_cols :].astype(jnp.bfloat16)
-    keys_values = jnp.concatenate([keys.reshape(tokens_here, key_cols), values], axis=1)
-    extended = padded(keys_values, (("sp", 0),), WINDOW)
+    values = kv_rows[:, key_cols:].astype(jnp.bfloat16)
+    extended = jnp.concatenate([keys.reshape(-1, key_cols), values], axis=1)
     sinks = sink_logit.reshape(heads_kv, group_size)
     biases = context_bias.reshape(heads_kv, group_size)
     block_rows = min(512, tokens_here)
@@ -203,8 +221,16 @@
         )
         outputs.append(block_out.reshape(block_rows, query_cols))
     attended = jnp.concatenate(outputs, axis=0)
-    projected = jnp.dot(
-        gathered_copies(attended, "tp", 1), out_weight, preferred_element_type=jnp.float32
+    core = column_index % CORES
+    weight_by_core = out_weight.reshape(-1, CORES, query_cols, column_count)
+    own_core_weight = lax.dynamic_index_in_dim(weight_by_core, core, 1, keepdims=False)
+    other_core_weight = lax.dynamic_index_in_dim(weight_by_core, 1 - core, 1, keepdims=False)
+    from_chips = same_core_copies(attended, "tp")
+    from_other = swapped_cores(from_chips, "tp")
+    projected = jnp.einsum(
+        "xrk,xkn->rn", from_chips, own_core_weight, preferred_element_type=jnp.float32
+    ) + jnp.einsum(
+        "xrk,xkn->rn", from_other, other_core_weight, preferred_element_type=jnp.float32
     )
     own_columns = lax.dynamic_slice_in_dim(latent, column_index * column_count, column_count, 1)
     gate_columns = lax.dynamic_slice_in_dim(

time: 121 us -> 125 us (1.033)
  waiting for transfers between devices: 39.6 us -> 5.24 us
  blocking collectives: 0 us -> 14.5 us
  other arithmetic: 12.5 us -> 22 us
  starting transfers between devices: 40.3 us -> 48 us
  local copies, waits for them, and re-layouts: 6.66 us -> 11.2 us
  matrix products: 20.3 us -> 23 us
    all_to_all x4 -> x3, waiting for transfers between devices: 36.2 us -> 3.51 us  [copy_for_each(): return lax.all_to_all(copies, axis, split_axis=0, concat_axis=0, tiled=True)]
    all_to_all x0 -> x1, blocking collectives: none -> 14.5 us  [same_core_copies(): lax.all_to_all(copies, axis, split_axis=0, concat_axis=0, tiled=True, axi...]
    ppermute x2 -> x3, starting transfers between devices: 4.28 us -> 10.2 us  [the longest x1 5.84 us: swapped_cores(): return lax.ppermute(block, axis, [(i, i ^ 1) for i in range(count)])]
    rsqrt x2 -> x3, other arithmetic: 0.02 us -> 3.13 us  [modulate(): normed = (values_f - center) * lax.rsqrt(spread + norm_eps)]
    reduce_sum x2 -> x3, other arithmetic: 2.42 us -> 5.2 us  [modulate(): spread = jnp.mean(jnp.square(values_f - center), -1, keepdims=True)]
    unnamed x22 -> x41, local copies, waits for them, and re-layouts: 2.68 us -> 5.27 us
    slice x2 -> x5, local copies, waits for them, and re-layouts: 0.05 us -> 2.61 us  [the longest x1 2.34 us: neighbour_rows(): low = lax.ppermute(rows[rows.shape[0] - width:], axis, forward)]
    and x2, other arithmetic: 1.52 us -> 3.85 us  [on_device(): (jnp.abs(query_pos[:, None] - key_pos[None, :]) <= WINDOW) & (key_pos >=...]
  transfers between devices with their start and end apart: 6 -> 6, of which waited for: 4 -> 2; matrix products, arithmetic and copies ran while one was open for 13% -> 29% of each run, Pallas kernels for 0% -> 0%
where the time goes in v1:
time: 125 us
  starting transfers between devices  48 us (38%)
  matrix products  23 us (18%)
  other arithmetic  22 us (18%)
  blocking collectives  14.5 us (12%)
  local copies, waits for them, and re-layouts  11.2 us (9%)
  waiting for transfers between devices  5.24 us (4%)
    all_to_all x3, starting transfers between devices, copy_for_each(): return lax.all_to_all(copies, axis, split_axis=0, concat_axis=0, tiled=True)  37.8 us
    all_to_all x1, blocking collectives, same_core_copies(): lax.all_to_all(copies, axis, split_axis=0, concat_axis=0, tiled=True, axi...  14.5 us
    ppermute x1, starting transfers between devices, swapped_cores(): return lax.ppermute(block, axis, [(i, i ^ 1) for i in range(count)])  5.84 us
    unnamed x41, local copies, waits for them, and re-layouts  5.27 us
    reduce_sum x3, other arithmetic, modulate(): spread = jnp.mean(jnp.square(values_f - center), -1, keepdims=True)  5.2 us
    dot_general x2, matrix products, attend_block(): jnp.einsum('qgrd,kgd->grqk', block_queries, block_keys, preferred_element...  4.96 us
    dot_general x1, matrix products, on_device(): jnp.dot(normed, merged_weight, preferred_element_type=jnp.float32)  4.64 us
    and x2, other arithmetic, on_device(): (jnp.abs(query_pos[:, None] - key_pos[None, :]) <= WINDOW) & (key_pos >=...  3.85 us
  transfers between devices with their start and end apart: 6, of which 2 were waited for; matrix products, arithmetic and copies ran while one was open for 29% of the time, Pallas kernels for 0%

profile of v1, /device:TPU:1, one launch (start us, length us, event | category | flops | bytes accessed | tf_op | source)
XLA Modules:
  0.0 124.5 jit_solution(4702241912636781728)
XLA Ops:
  1.9 17.1 %all-to-all-start = ((f32[64,2,3,256]{3,1,2,0:T(2,128)}), f32[64,2,3,256]{3,1,2,0:T(2,128)S(1)}, u32[]{:S(2)}, u32[]{:S(2)}) async-start(f32[64,2,3,256]{3,1,2,0:T(2,128)} %broadcast_in_dim.18), calls=%async_computation | async-start | bytes 786432 | tf_op jit(solution)/shard_map/all_to_all | solution.py:18
  19.0 2.3 %fusion.131 = (bf16[128,2048]{1,0:T(8,128)(2,1)}, bf16[128,2048]{1,0:T(8,128)(2,1)}) fusion(bf16[1024,2048]{1,0:T(8,128)(2,1)} %param.11), kind=kLoop, calls=%fused_computation.193 | loop fusion | bytes 2097152 | tf_op jit(solution)/shard_map/slice | solution.py:40
  21.4 3.1 %collective-permute-start = (bf16[128,2048]{1,0:T(8,128)(2,1)}, bf16[128,2048]{1,0:T(8,128)(2,1)S(1)}, u32[]{:S(2)}, u32[]{:S(2)}) collective-permute-start(bf16[128,2048]{1,0:T(8,128)(2,1)} %get-tuple-element.7), channel_id=1, source_target_pairs={{0,8},{8,16},{16,24},{24,32},{32,40},{40,48},{48,56},{56,64},{64,7... | collective-permute-start | bytes 1572872 | tf_op jit(solution)/shard_map/ppermute | solution.py:40
  24.4 1.3 %collective-permute-start.1 = (bf16[128,2048]{1,0:T(8,128)(2,1)}, bf16[128,2048]{1,0:T(8,128)(2,1)S(1)}, u32[]{:S(2)}, u32[]{:S(2)}) collective-permute-start(bf16[128,2048]{1,0:T(8,128)(2,1)} %get-tuple-element.8), channel_id=1, source_target_pairs={{8,0},{16,8},{24,16},{32,24},{40,32},{48,40},{56,48},{64,56},{72,6... | collective-permute-start | bytes 1572872 | tf_op jit(solution)/shard_map/ppermute | solution.py:41
  26.4 2.8 %convert_reduce_fusion = f32[1024]{0:T(1024)S(1)} fusion(bf16[1024,2048]{1,0:T(8,128)(2,1)} %param.11), kind=kLoop, calls=%fused_computation.1 | loop fusion | flops 4193280 | bytes 4198400 | tf_op jit(solution)/shard_map/reduce_sum | solution.py:83
  33.1 3.4 %fusion.2 = f32[1024]{0:T(1024)S(1)} fusion(bf16[1024,2048]{1,0:T(8,128)(2,1)} %param.11, f32[1024]{0:T(1024)S(1)} %broadcast_multiply_fusion.2), kind=kLoop, calls=%fused_computation.4 | loop fusion | flops 8387584 | bytes 4202496 | tf_op jit(solution)/shard_map/reduce_sum | solution.py:84
  40.0 1.6 %fusion.31 = pred[512,768]{0,1:T(8,128)(4,1)S(1)} fusion(s32[768]{0:T(1024)S(1)} %iota_add_fusion.2, s32[512]{0:T(512)S(1)} %iota_add_fusion.4, pred[768]{0:T(1024)(128)(4,1)} %get-tuple-element.40, pred[768]{0:T(1024)(128)(4,1)} %get-tuple-element.41), kind=kLoop, calls=%fused_computation.50 | loop fusion | flops 1966080 | bytes 399872 | tf_op jit(solution)/shard_map/and | solution.py:208
  41.6 1.2 %add_rsqrt_fusion.2 = f32[16]{0:T(128)} fusion(f32[16]{0:T(128)} %fusion.67), kind=kLoop, calls=%fused_computation.174 | loop fusion | flops 32 | bytes 128 | tf_op jit(solution)/shard_map/rsqrt | solution.py:85
  42.8 2.3 %fusion.33 = pred[512,768]{0,1:T(8,128)(4,1)} fusion(s32[768]{0:T(1024)S(1)} %iota_add_fusion.1, s32[512]{0:T(512)S(1)} %iota_add_fusion.3, pred[768]{0:T(1024)(128)(4,1)} %get-tuple-element.42, pred[768]{0:T(1024)(128)(4,1)} %get-tuple-element.43), kind=kLoop, calls=%fused_computation.52 | loop fusion | flops 1966080 | bytes 399872 | tf_op jit(solution)/shard_map/and | solution.py:208
  47.1 5.8 %all-to-all-start.1 = ((f32[8,2,3,256]{3,1,2,0:T(2,128)}), f32[8,2,3,256]{3,1,2,0:T(2,128)S(1)}, u32[]{:S(2)}, u32[]{:S(2)}) async-start(f32[8,2,3,256]{3,1,2,0:T(2,128)} %broadcast_in_dim.19), calls=%async_computation.1 | async-start | bytes 98304 | tf_op jit(solution)/shard_map/all_to_all | solution.py:18
  52.9 1.3 %add_rsqrt_fusion.1 = f32[256]{0:T(256)} fusion(f32[256]{0:T(256)} %fusion.18), kind=kLoop, calls=%fused_computation.165 | loop fusion | flops 512 | bytes 2048 | tf_op jit(solution)/shard_map/rsqrt | solution.py:85
  54.2 3.5 %all-to-all-done.1 = f32[8,2,3,256]{3,1,2,0:T(2,128)S(1)} async-done(((f32[8,2,3,256]{3,1,2,0:T(2,128)}), f32[8,2,3,256]{3,1,2,0:T(2,128)S(1)}, u32[]{:S(2)}, u32[]{:S(2)}) %all-to-all-start.1) | async-done | bytes 49184 | tf_op jit(solution)/shard_map/all_to_all | solution.py:18
  57.8 1.4 %convolution_convert_fusion = bf16[16,128]{1,0:T(8,128)(2,1)S(1)} fusion(bf16[2048,128]{0,1:T(8,128)(2,1)} %constant_dynamic-update-slice_fusion, bf16[16,2048]{1,0:T(8,128)(2,1)} %param.12, f32[2048]{0:T(1024)S(1)} %bitcast.216, f32[2048]{0:T(1024)S(1)} %bitcast.215, f32[16]{0:T(128)} %add_rsqrt_fusion.2, f32[16]{0:T(128)} %copy-done.18), kind=kOutput, calls=%fused_computation.63 | convolution fusion | flops 8587264 | bytes 610432 | tf_op jit(solution)/shard_map/dot_general | solution.py:161
  59.9 14.9 %all-to-all-start.2 = ((bf16[64,16,128]{2,1,0:T(8,128)(2,1)}), bf16[64,16,128]{2,1,0:T(8,128)(2,1)S(1)}, u32[]{:S(2)}, u32[]{:S(2)}) async-start(bf16[64,16,128]{2,1,0:T(8,128)(2,1)} %broadcast_in_dim.22), calls=%async_computation.2 | async-start | bytes 524288 | tf_op jit(solution)/shard_map/all_to_all | solution.py:18
  74.8 4.6 %fusion.8 = f32[1024,256]{0,1:T(8,128)S(1)} fusion(bf16[1024,2048]{1,0:T(8,128)(2,1)} %param.11, f32[2048]{0:T(1024)S(1)} %bitcast.213, f32[2048]{0:T(1024)S(1)} %bitcast.211, f32[1024]{0:T(1024)} %add_rsqrt_fusion, f32[1024]{0:T(1024)S(1)} %broadcast_multiply_fusion.2, bf16[2048,64]{1,0:T(8,128)(2,1)S(1)} %copy.41, bf16[2048,64]{1,0:T(8,128)(2,1)S(1)} %copy-done.6, ...), kind=kOutput, calls=%fused_computation.18 | convolution fusion | flops 1089470464 | bytes 6316032 | tf_op jit(solution)/shard_map/dot_general | solution.py:170
  79.6 1.3 %fusion.55 = f32[256,128]{1,0:T(8,128)S(1)} fusion(bf16[2048,128]{0,1:T(8,128)(2,1)S(1)} %copy-done.13, f32[2048]{0:T(1024)} %bitcast.214, f32[2048]{0:T(1024)S(1)} %bitcast.212, f32[256]{0:T(256)S(1)} %copy-done.17, f32[256]{0:T(256)S(1)} %broadcast_multiply_fusion.3, bf16[128,2048]{1,0:T(8,128)(2,1)S(1)} %collective-permute-done.1, ...), kind=kOutput, calls=%fused_computation.70 | convolution fusion | flops 138936320 | bytes 1722368 | tf_op jit(solution)/shard_map/dot_general | solution.py:171
  82.4 2.5 %fusion.17 = (f32[2,512]{1,0:T(2,128)S(1)}, f32[768,512,2]{1,0,2:T(8,128)}) fusion(pred[512,768]{0,1:T(8,128)(4,1)S(1)} %copy-done.3, bf16[1024,2,32]{0,2,1:T(8,128)(2,1)S(1)} %get-tuple-element.12, bf16[1024,2,32]{0,2,1:T(8,128)(2,1)S(1)} %get-tuple-element.11, bf16[1280,32]{0,1:T(8,128)(2,1)S(1)} %get-tuple-element.14, ...), kind=kOutput, calls=%fused_computation.34 | convolution fusion | flops 103480320 | bytes 3969024 | tf_op jit(solution)/shard_map/qgrd,kgd->grqk/dot_general | solution.py:109
  84.9 2.5 %fusion.16 = (f32[2,512]{1,0:T(2,128)S(1)}, f32[768,512,2]{1,0,2:T(8,128)}) fusion(pred[512,768]{0,1:T(8,128)(4,1)S(1)} %fusion.31, bf16[1024,2,32]{0,2,1:T(8,128)(2,1)S(1)} %get-tuple-element.11, bf16[1024,2,32]{0,2,1:T(8,128)(2,1)S(1)} %get-tuple-element.12, bf16[1280,32]{0,1:T(8,128)(2,1)S(1)} %get-tuple-element.13, ...), kind=kOutput, calls=%fused_computation.33 | convolution fusion | flops 103480320 | bytes 3969024 | tf_op jit(solution)/shard_map/qgrd,kgd->grqk/dot_general | solution.py:109
  90.1 1.4 %fusion.10 = (f32[2,512]{1,0:T(2,128)S(1)}, f32[2,512]{1,0:T(2,128)S(1)}, f32[1024,512,2]{1,0,2:T(8,128)S(1)}) fusion(f32[1024,512,2]{1,0,2:T(8,128)S(1)} %get-tuple-element.34, f32[2,512]{1,0:T(2,128)S(1)} %maximum_maximum_fusion.1, f32[2]{0:T(128)S(1)} %copy-done.15, bf16[1024,2,32]{0,2,1:T(8,128)(2,1)S(1)} %get-tuple-element.12, ...), kind=kOutput, calls=%fused_computation.19 | convolution fusion | flops 141817856 | bytes 8925192 | tf_op jit(solution)/shard_map/qgrd,cgd->grqc/dot_general | solution.py:114
  96.8 1.3 %fusion.47 = bf16[64,2,512]{2,0,1:T(8,128)(2,1)S(1)} fusion(f32[64,2,512]{2,0,1:T(8,128)S(1)} %fusion.24, f32[2,512]{1,0:T(2,128)S(1)} %get-tuple-element.27, f32[2,512]{1,0:T(2,128)S(1)} %maximum_maximum_fusion.1, f32[768,512,2]{1,0,2:T(8,128)S(1)} %copy-done.2, pred[512,768]{0,1:T(8,128)(4,1)S(1)} %fusion.31, bf16[1280,128]{0,1:T(8,128)(2,1)S(1)} %fusion.130), kind=kOutput, calls=%fused_computation.62 | convolution fusion | flops 104726528 | bytes 4038656 | tf_op jit(solution)/shard_map/grqk,kgd->qgrd/dot_general | solution.py:121
  99.6 14.5 %all_to_all.20 = bf16[4,1024,128]{2,1,0:T(8,128)(2,1)S(1)} all-to-all(bf16[4,1024,128]{2,1,0:T(8,128)(2,1)S(1)} %broadcast_in_dim.24), channel_id=1, replica_groups={{0,2,4,6},{1,3,5,7},{8,10,12,14},{9,11,13,15},{16,18,20,22},{17,19,21,2..., dimensions={0} | all-to-all | bytes 2097152 | tf_op jit(solution)/shard_map/all_to_all | solution.py:49
  114.1 5.8 %collective-permute-start.2 = (bf16[4,1024,128]{2,1,0:T(8,128)(2,1)S(1)}, bf16[4,1024,128]{2,1,0:T(8,128)(2,1)S(1)}, u32[]{:S(2)}, u32[]{:S(2)}) collective-permute-start(bf16[4,1024,128]{2,1,0:T(8,128)(2,1)S(1)} %all_to_all.20), channel_id=1, source_target_pairs={{0,1},{1,0},{2,3},{3,2},{4,5},{5,4},{6,7},{7,6},{8,9},{9,8},{10,11... | collective-permute-start | bytes 3145736 | tf_op jit(solution)/shard_map/ppermute | solution.py:56
  120.5 1.7 %collective-permute-done.2 = bf16[4,1024,128]{2,1,0:T(8,128)(2,1)S(1)} collective-permute-done((bf16[4,1024,128]{2,1,0:T(8,128)(2,1)S(1)}, bf16[4,1024,128]{2,1,0:T(8,128)(2,1)S(1)}, u32[]{:S(2)}, u32[]{:S(2)}) %collective-permute-start.2) | collective-permute-done | bytes 1048608 | tf_op jit(solution)/shard_map/ppermute | solution.py:56
  122.3 2.3 %fusion.37 = bf16[1024,256]{1,0:T(8,128)(2,1)} fusion(f32[1024,256]{1,0:T(8,128)S(1)} %convolution_bitcast_fusion.1, bf16[4,1024,128]{2,1,0:T(8,128)(2,1)S(1)} %collective-permute-done.2, f32[256]{0:T(256)S(1)} %bitcast.217, bf16[1024,2048]{1,0:T(8,128)(2,1)} %param.11, s32[]{:T(128)S(6)} %select_n.44, bf16[4,2,128,256]{3,2,1,0:T(8,128)(2,1)S(1)} %bitcast.199, ...), kind=kOutput, calls=%fused_computation.58 | convolution fusion | flops 269746176 | bytes 3408904 | tf_op jit(solution)/shard_map/xrk,xkn->rn/dot_general | solution.py:232
  (96 shorter events, 24.1 us)
Async XLA Ops:
  0.0 120.1 %copy-start = (bf16[1024,256]{1,0:T(8,128)(2,1)S(1)}, bf16[1024,256]{1,0:T(8,128)(2,1)}, u32[]{:S(2)}) copy-start(bf16[1024,256]{1,0:T(8,128)(2,1)} %param.19) | copy-start | bytes 1572868
  1.9 44.5 %all-to-all-start = ((f32[64,2,3,256]{3,1,2,0:T(2,128)}), f32[64,2,3,256]{3,1,2,0:T(2,128)S(1)}, u32[]{:S(2)}, u32[]{:S(2)}) async-start(f32[64,2,3,256]{3,1,2,0:T(2,128)} %broadcast_in_dim.18), calls=%async_computation | async-start | bytes 786432 | tf_op jit(solution)/shard_map/all_to_all | solution.py:18
  19.0 10.8 %copy-start.4 = (bf16[2048,64]{0,1:T(8,128)(2,1)S(1)}, bf16[2048,64]{0,1:T(8,128)(2,1)}, u32[]{:S(2)}) copy-start(bf16[2048,64]{0,1:T(8,128)(2,1)} %param.17) | copy-start | bytes 786436
  21.4 10.2 %copy-start.12 = (bf16[16,2048]{1,0:T(8,128)(2,1)S(1)}, bf16[16,2048]{1,0:T(8,128)(2,1)}, u32[]{:S(2)}) copy-start(bf16[16,2048]{1,0:T(8,128)(2,1)} %param.12) | copy-start | bytes 196612
  21.4 23.7 %collective-permute-start = (bf16[128,2048]{1,0:T(8,128)(2,1)}, bf16[128,2048]{1,0:T(8,128)(2,1)S(1)}, u32[]{:S(2)}, u32[]{:S(2)}) collective-permute-start(bf16[128,2048]{1,0:T(8,128)(2,1)} %get-tuple-element.7), channel_id=1, source_target_pairs={{0,8},{8,16},{16,24},{24,32},{32,40},{40,48},{48,56},{56,64},{64,7... | collective-permute-start | bytes 1572872 | tf_op jit(solution)/shard_map/ppermute | solution.py:40
  24.4 20.7 %collective-permute-start.1 = (bf16[128,2048]{1,0:T(8,128)(2,1)}, bf16[128,2048]{1,0:T(8,128)(2,1)S(1)}, u32[]{:S(2)}, u32[]{:S(2)}) collective-permute-start(bf16[128,2048]{1,0:T(8,128)(2,1)} %get-tuple-element.8), channel_id=1, source_target_pairs={{8,0},{16,8},{24,16},{32,24},{40,32},{48,40},{56,48},{64,56},{72,6... | collective-permute-start | bytes 1572872 | tf_op jit(solution)/shard_map/ppermute | solution.py:41
  29.2 7.9 %copy-start.5 = (bf16[2048,64]{0,1:T(8,128)(2,1)S(1)}, bf16[2048,64]{0,1:T(8,128)(2,1)}, u32[]{:S(2)}) copy-start(bf16[2048,64]{0,1:T(8,128)(2,1)} %param.18) | copy-start | bytes 786436
  38.1 36.7 %copy-start.6 = (bf16[2048,64]{1,0:T(8,128)(2,1)S(1)}, bf16[2048,64]{1,0:T(8,128)(2,1)}, u32[]{:S(2)}) copy-start(bf16[2048,64]{1,0:T(8,128)(2,1)} %copy.40) | copy-start | bytes 786436
  47.1 10.6 %all-to-all-start.1 = ((f32[8,2,3,256]{3,1,2,0:T(2,128)}), f32[8,2,3,256]{3,1,2,0:T(2,128)S(1)}, u32[]{:S(2)}, u32[]{:S(2)}) async-start(f32[8,2,3,256]{3,1,2,0:T(2,128)} %broadcast_in_dim.19), calls=%async_computation.1 | async-start | bytes 98304 | tf_op jit(solution)/shard_map/all_to_all | solution.py:18
  57.7 2.2 %copy-start.8 = (f32[8,2,3,256]{3,1,2,0:T(2,128)}, f32[8,2,3,256]{3,1,2,0:T(2,128)S(1)}, u32[]{:S(2)}) copy-start(f32[8,2,3,256]{3,1,2,0:T(2,128)S(1)} %all-to-all-done.1) | copy-start | bytes 147460
  57.8 17.0 %copy-start.14 = (f32[1,1,8,256]{3,0,1,2:T(1,128)}, f32[1,1,8,256]{3,0,1,2:T(1,128)S(1)}, u32[]{:S(2)}) copy-start(f32[1,1,8,256]{3,0,1,2:T(1,128)S(1)} %get-tuple-element.21) | copy-start | bytes 24580
  59.9 27.5 %all-to-all-start.2 = ((bf16[64,16,128]{2,1,0:T(8,128)(2,1)}), bf16[64,16,128]{2,1,0:T(8,128)(2,1)S(1)}, u32[]{:S(2)}, u32[]{:S(2)}) async-start(bf16[64,16,128]{2,1,0:T(8,128)(2,1)} %broadcast_in_dim.22), calls=%async_computation.2 | async-start | bytes 524288 | tf_op jit(solution)/shard_map/all_to_all | solution.py:18
  74.8 4.8 %copy-start.13 = (bf16[2048,128]{0,1:T(8,128)(2,1)S(1)}, bf16[2048,128]{0,1:T(8,128)(2,1)}, u32[]{:S(2)}) copy-start(bf16[2048,128]{0,1:T(8,128)(2,1)} %constant_dynamic-update-slice_fusion) | copy-start | bytes 1572868
  74.8 4.8 %copy-start.17 = (f32[256]{0:T(256)S(1)}, f32[256]{0:T(256)}, u32[]{:S(2)}) copy-start(f32[256]{0:T(256)} %add_rsqrt_fusion.1) | copy-start | bytes 3076
  79.6 1.7 %copy-start.7 = (f32[1024,32]{0,1:T(8,128)S(1)}, f32[1024,32]{0,1:T(8,128)}, u32[]{:S(2)}) copy-start(f32[1024,32]{0,1:T(8,128)} %get-tuple-element.16) | copy-start | bytes 393220
  80.9 0.9 copy-start.10
  80.9 0.9 copy-start.11
  80.9 1.5 %copy-start.3 = (pred[512,768]{0,1:T(8,128)(4,1)S(1)}, pred[512,768]{0,1:T(8,128)(4,1)}, u32[]{:S(2)}) copy-start(pred[512,768]{0,1:T(8,128)(4,1)} %fusion.33) | copy-start | bytes 1179652
  84.9 2.6 %copy-start.15 = (f32[2]{0:T(128)S(1)}, f32[2]{0:T(128)}, u32[]{:S(2)}) copy-start(f32[2]{0:T(128)} %param.21) | copy-start | bytes 28
  87.4 0.7 copy-start.16
  87.4 1.9 %copy-start.2 = (f32[768,512,2]{1,0,2:T(8,128)S(1)}, f32[768,512,2]{1,0,2:T(8,128)}, u32[]{:S(2)}) copy-start(f32[768,512,2]{1,0,2:T(8,128)} %get-tuple-element.32) | copy-start | bytes 9437188
  92.9 1.9 %copy-start.1 = (f32[768,512,2]{1,0,2:T(8,128)S(1)}, f32[768,512,2]{1,0,2:T(8,128)}, u32[]{:S(2)}) copy-start(f32[768,512,2]{1,0,2:T(8,128)} %get-tuple-element.37) | copy-start | bytes 9437188
  99.3 20.8 %copy-start.9 = (f32[8,2,3,256]{3,1,2,0:T(2,128)S(1)}, f32[8,2,3,256]{3,1,2,0:T(2,128)}, u32[]{:S(2)}) copy-start(f32[8,2,3,256]{3,1,2,0:T(2,128)} %copy-done.8) | copy-start | bytes 147460
  114.1 8.1 %collective-permute-start.2 = (bf16[4,1024,128]{2,1,0:T(8,128)(2,1)S(1)}, bf16[4,1024,128]{2,1,0:T(8,128)(2,1)S(1)}, u32[]{:S(2)}, u32[]{:S(2)}) collective-permute-start(bf16[4,1024,128]{2,1,0:T(8,128)(2,1)S(1)} %all_to_all.20), channel_id=1, source_target_pairs={{0,1},{1,0},{2,3},{3,2},{4,5},{5,4},{6,7},{7,6},{8,9},{9,8},{10,11... | collective-permute-start | bytes 3145736 | tf_op jit(solution)/shard_map/ppermute | solution.py:56
  (1 other events, 0.6 us)

commit v2 on v1

v2 whole, which is shorter than its diff:
```python
import functools

import jax
import jax.numpy as jnp
from jax import lax
from jax.experimental import pallas as pl
from jax.experimental.pallas import tpu as pltpu
from jax.sharding import PartitionSpec as P

HEAD_DIM = 64
WINDOW = 128
GRID_W = 64
CORES = 2
STEP_ROWS = 2 * WINDOW
NORM_ROWS = 16


norm_eps = 1e-05
rope_base = 10000.0


def copy_for_each(shard, axis):
    copies = jnp.broadcast_to(shard, (lax.axis_size(axis), *shard.shape))
    return lax.all_to_all(copies, axis, split_axis=0, concat_axis=0, tiled=True)


def of_everyone(shard, axis):
    everything = copy_for_each(shard, axis)
    return jnp.sum(everything, axis=0)


def joined_along(parts, dim):
    dims = list(parts.shape[1:])
    dims[dim] *= parts.shape[0]
    return jnp.moveaxis(parts, 0, dim).reshape(dims)


def gathered_copies(shard, axis, dim):
    return joined_along(copy_for_each(shard, axis), dim)


def neighbour_rows(rows, width, axis):
    count = lax.axis_size(axis)
    forward = [(i, i + 1) for i in range(count - 1)]
    backward = [(target, source) for source, target in forward]
    low = lax.ppermute(rows[rows.shape[0] - width :], axis, forward)
    high = lax.ppermute(rows[:width], axis, backward)
    return jnp.concatenate([low, high], axis=0)


def from_same_cores(copies, axis):
    count = lax.axis_size(axis)
    groups = [list(range(core, count, CORES)) for core in range(CORES)]
    return lax.all_to_all(
        copies, axis, split_axis=0, concat_axis=0, tiled=True, axis_index_groups=groups
    )


def swapped_cores(block, axis):
    count = lax.axis_size(axis)
    return lax.ppermute(block, axis, [(i, i ^ 1) for i in range(count)])


def rotary_tables(positions):
    grid_row = (positions // GRID_W).astype(jnp.float32)
    grid_col = (positions % GRID_W).astype(jnp.float32)
    freq_count = HEAD_DIM // 4
    inverse = rope_base ** (-jnp.arange(freq_count, dtype=jnp.float32) / freq_count)
    angles = jnp.concatenate([grid_row[:, None] * inverse, grid_col[:, None] * inverse], axis=-1)
    return (jnp.cos(angles), jnp.sin(angles))


def modulate(row_block, shift_scale):
    values_f = row_block.astype(jnp.float32)
    center = jnp.mean(values_f, -1, keepdims=True)
    spread = jnp.mean(jnp.square(values_f - center), -1, keepdims=True)
    normed = (values_f - center) * lax.rsqrt(spread + norm_eps)
    return (normed * (1.0 + shift_scale[1]) + shift_scale[0]).astype(jnp.bfloat16)


def rotated_columns(vectors, cos_table, sin_table):
    half_dim = vectors.shape[0] // 2
    first_half = vectors[:half_dim]
    second_half = vectors[half_dim:]
    return jnp.concatenate(
        [
            first_half * cos_table - second_half * sin_table,
            first_half * sin_table + second_half * cos_table,
        ],
        axis=0,
    )


def window_kernel(
    start_ref,
    latent_ref,
    halo_ref,
    weight_ref,
    shift_ref,
    gain_ref,
    cos_ref,
    sin_ref,
    queries_ref,
    partial_ref,
    stats_ref,
    normed_ref,
    keys_ref,
    values_ref,
    *,
    tokens,
    seq_total,
):
    step = pl.program_id(0)
    own_steps = tokens // STEP_ROWS
    width = weight_ref.shape[1]
    group = weight_ref.shape[0] // HEAD_DIM - 2
    lanes = group * WINDOW

    def project(rows_ref):
        def normalise(index, carry):
            first = pl.multiple_of(index * NORM_ROWS, NORM_ROWS)
            rows = rows_ref[pl.ds(first, NORM_ROWS), :].astype(jnp.float32)
            center = jnp.sum(rows, axis=1, keepdims=True) * (1.0 / width)
            rows = rows - center
            spread = jnp.sum(rows * rows, axis=1, keepdims=True) * (1.0 / width)
            rows = rows * lax.rsqrt(spread + norm_eps)
            normed_ref[pl.ds(first, NORM_ROWS), :] = (
                rows * gain_ref[...] + shift_ref[...]
            ).astype(jnp.bfloat16)
            return carry

        lax.fori_loop(0, STEP_ROWS // NORM_ROWS, normalise, 0, unroll=2)
        return lax.dot_general(
            weight_ref[...],
            normed_ref[...],
            (((1,), (1,)), ((), ())),
            preferred_element_type=jnp.float32,
        )

    def keys_of(columns, cos_table, sin_table):
        rotated = rotated_columns(columns, cos_table, sin_table)
        return jnp.transpose(rotated).astype(jnp.bfloat16)

    key_row = group * HEAD_DIM
    value_row = key_row + HEAD_DIM

    @pl.when(step < own_steps)
    def _():
        columns = project(latent_ref)
        first = pl.multiple_of(WINDOW + step * STEP_ROWS, WINDOW)
        cos_table = cos_ref[:, pl.ds(first, STEP_ROWS)]
        sin_table = sin_ref[:, pl.ds(first, STEP_ROWS)]
        keys_ref[pl.ds(first, STEP_ROWS), :] = keys_of(
            columns[key_row:value_row], cos_table, sin_table
        )
        values = columns[value_row:].astype(jnp.bfloat16)
        values_ref[:, pl.ds(first, STEP_ROWS)] = values
        for head in range(group):
            rotated = rotated_columns(
                columns[head * HEAD_DIM : (head + 1) * HEAD_DIM], cos_table, sin_table
            )
            rotated = rotated.astype(jnp.bfloat16) * jnp.bfloat16(HEAD_DIM**-0.5)
            for part in range(STEP_ROWS // WINDOW):
                queries_ref[
                    step * (STEP_ROWS // WINDOW) + part, :, head * WINDOW : (head + 1) * WINDOW
                ] = rotated[:, part * WINDOW : (part + 1) * WINDOW]

    @pl.when(step == own_steps)
    def _():
        columns = project(halo_ref)
        last = WINDOW + tokens
        for first, part in ((0, 0), (last, WINDOW)):
            here = columns[:, part : part + WINDOW]
            keys_ref[first : first + WINDOW, :] = keys_of(
                here[key_row:value_row],
                cos_ref[:, first : first + WINDOW],
                sin_ref[:, first : first + WINDOW],
            )
            values_ref[:, first : first + WINDOW] = here[value_row:].astype(jnp.bfloat16)
        span = 3 * WINDOW
        key_index = lax.broadcasted_iota(jnp.int32, (span, lanes), 0)
        query_index = lax.broadcasted_iota(jnp.int32, (span, lanes), 1) % WINDOW
        band = (key_index >= query_index) & (key_index <= query_index + 2 * WINDOW)

        def attend(block, carry):
            row = pl.multiple_of(block * WINDOW, WINDOW)
            key_start = start_ref[0] + row - WINDOW
            scores = jnp.dot(
                keys_ref[pl.ds(row, span), :],
                queries_ref[block],
                preferred_element_type=jnp.float32,
            )
            valid = band & (key_index >= -key_start) & (key_index < seq_total - key_start)
            scores = jnp.where(valid, scores, -jnp.inf)
            top = jnp.max(scores, axis=0, keepdims=True)
            weights = jnp.exp(scores - top)
            stats_ref[block, 0:1, :] = top
            stats_ref[block, 1:2, :] = jnp.sum(weights, axis=0, keepdims=True)
            partial_ref[block] = jnp.dot(
                values_ref[:, pl.ds(row, span)],
                weights.astype(jnp.bfloat16),
                preferred_element_type=jnp.float32,
            )
            return carry

        lax.fori_loop(0, tokens // WINDOW, attend, 0)


def context_kernel(
    queries_ref, partial_ref, stats_ref, context_ref, sink_ref, bias_ref, out_ref, values_ref
):
    group = queries_ref.shape[2] // WINDOW

    @pl.when(pl.program_id(0) == 0)
    def _():
        both = jnp.transpose(context_ref[...].astype(jnp.float32))
        values_ref[...] = both[HEAD_DIM:].astype(jnp.bfloat16)

    scores = jnp.dot(
        context_ref[:, :HEAD_DIM], queries_ref[0], preferred_element_type=jnp.float32
    )
    bias = bias_ref[...]
    sink = sink_ref[...]
    window_top = stats_ref[0, 0:1, :]
    top = jnp.maximum(
        jnp.maximum(jnp.max(scores, axis=0, keepdims=True) + bias, window_top), sink
    )
    weights = jnp.exp(scores - (top - bias))
    window_share = jnp.exp(window_top - top)
    total = (
        jnp.sum(weights, axis=0, keepdims=True)
        + stats_ref[0, 1:2, :] * window_share
        + jnp.exp(sink - top)
    )
    mixed = (
        jnp.dot(values_ref[...], weights.astype(jnp.bfloat16), preferred_element_type=jnp.float32)
        + partial_ref[0] * window_share
    )
    mixed = mixed / total
    heads = [mixed[:, head * WINDOW : (head + 1) * WINDOW] for head in range(group)]
    rows = jnp.transpose(jnp.concatenate(heads, axis=0)).astype(jnp.bfloat16)
    for copy in range(out_ref.shape[0]):
        out_ref[copy] = rows


def on_device(
    latent,
    context,
    cond_lat,
    cond_ctx,
    mod_weight,
    query_weight,
    key_weight,
    value_weight,
    out_weight,
    sink_logit,
    context_bias,
):
    tokens_here = latent.shape[0]
    column_count = out_weight.shape[1]
    column_index = lax.axis_index("tp")
    query_cols = query_weight.shape[1]
    key_cols = key_weight.shape[1]
    group_size = query_cols // key_cols
    activated = jax.nn.silu(jnp.stack([cond_lat, cond_ctx]).astype(jnp.float32)).astype(
        jnp.bfloat16
    )
    partial_mod = jnp.einsum(
        "cd,rde->cre", activated, mod_weight, preferred_element_type=jnp.float32
    )
    halo_rows = neighbour_rows(latent, WINDOW, "sp")
    summed_mod = of_everyone(partial_mod, "sp")
    modulation = gathered_copies(summed_mod, "tp", 2)
    kv_weight = jnp.concatenate([key_weight, value_weight], axis=1)
    context_normed = modulate(context, modulation[1])
    context_kv = gathered_copies(
        jnp.dot(context_normed, kv_weight, preferred_element_type=jnp.float32).astype(jnp.bfloat16),
        "sp",
        0,
    )
    offset = lax.axis_index("sp") * tokens_here
    seq_total = tokens_here * lax.axis_size("sp")
    positions = offset - WINDOW + jnp.arange(tokens_here + 2 * WINDOW, dtype=jnp.int32)
    cos_table, sin_table = rotary_tables(positions)
    weight_rows = jnp.concatenate([query_weight.T, key_weight.T, value_weight.T], axis=0)
    own_steps = tokens_here // STEP_ROWS
    blocks = tokens_here // WINDOW
    lanes = group_size * WINDOW
    features = latent.shape[1]
    whole = lambda *shape: pl.BlockSpec(shape, lambda i: (0,) * len(shape))
    queries, partial, stats = pl.pallas_call(
        functools.partial(window_kernel, tokens=tokens_here, seq_total=seq_total),
        grid=(own_steps + 1,),
        in_specs=[
            pl.BlockSpec(memory_space=pltpu.SMEM),
            pl.BlockSpec((STEP_ROWS, features), lambda i: (jnp.minimum(i, own_steps - 1), 0)),
            whole(STEP_ROWS, features),
            whole(*weight_rows.shape),
            whole(1, features),
            whole(1, features),
            whole(HEAD_DIM // 2, tokens_here + 2 * WINDOW),
            whole(HEAD_DIM // 2, tokens_here + 2 * WINDOW),
        ],
        out_specs=[
            whole(blocks, HEAD_DIM, lanes),
            whole(blocks, HEAD_DIM, lanes),
            whole(blocks, 8, lanes),
        ],
        out_shape=[
            jax.ShapeDtypeStruct((blocks, HEAD_DIM, lanes), jnp.bfloat16),
            jax.ShapeDtypeStruct((blocks, HEAD_DIM, lanes), jnp.float32),
            jax.ShapeDtypeStruct((blocks, 8, lanes), jnp.float32),
        ],
        scratch_shapes=[
            pltpu.VMEM((STEP_ROWS, features), jnp.bfloat16),
            pltpu.VMEM((tokens_here + 2 * WINDOW, HEAD_DIM), jnp.bfloat16),
            pltpu.VMEM((HEAD_DIM, tokens_here + 2 * WINDOW), jnp.bfloat16),
        ],
        name="window_part",
    )(
        offset.reshape(1),
        latent,
        halo_rows,
        weight_rows,
        modulation[0, 0][None],
        1.0 + modulation[0, 1][None],
        cos_table.T,
        sin_table.T,
    )
    chips = lax.axis_size("tp") // CORES
    attended = pl.pallas_call(
        context_kernel,
        grid=(blocks,),
        in_specs=[
            pl.BlockSpec((1, HEAD_DIM, lanes), lambda i: (i, 0, 0)),
            pl.BlockSpec((1, HEAD_DIM, lanes), lambda i: (i, 0, 0)),
            pl.BlockSpec((1, 8, lanes), lambda i: (i, 0, 0)),
            whole(*context_kv.shape),
            whole(1, lanes),
            whole(1, lanes),
        ],
        out_specs=pl.BlockSpec((chips, WINDOW, query_cols), lambda i: (0, i, 0)),
        out_shape=jax.ShapeDtypeStruct((chips, tokens_here, query_cols), jnp.bfloat16),
        scratch_shapes=[pltpu.VMEM((HEAD_DIM, context_kv.shape[0]), jnp.bfloat16)],
        name="context_part",
    )(
        queries,
        partial,
        stats,
        context_kv,
        jnp.repeat(sink_logit, WINDOW)[None],
        jnp.repeat(context_bias, WINDOW)[None],
    )
    core = column_index % CORES
    weight_by_core = out_weight.reshape(-1, CORES, query_cols, column_count)
    own_core_weight = lax.dynamic_index_in_dim(weight_by_core, core, 1, keepdims=False)
    other_core_weight = lax.dynamic_index_in_dim(weight_by_core, 1 - core, 1, keepdims=False)
    from_chips = from_same_cores(attended, "tp")
    from_other = swapped_cores(from_chips, "tp")
    projected = jnp.einsum(
        "xrk,xkn->rn", from_chips, own_core_weight, preferred_element_type=jnp.float32
    ) + jnp.einsum(
        "xrk,xkn->rn", from_other, other_core_weight, preferred_element_type=jnp.float32
    )
    own_columns = lax.dynamic_slice_in_dim(latent, column_index * column_count, column_count, 1)
    gate_columns = lax.dynamic_slice_in_dim(
        modulation[0, 2], column_index * column_count, column_count, 0
    )
    return (own_columns.astype(jnp.float32) + gate_columns * projected).astype(jnp.bfloat16)


def solution(mesh):
    return jax.shard_map(
        on_device,
        mesh=mesh,
        in_specs=(
            P("sp", None),
            P("sp", None),
            P("sp"),
            P("sp"),
            P(None, "sp", "tp"),
            P(None, "tp"),
            P(None, "tp"),
            P(None, "tp"),
            P(None, "tp"),
            P("tp"),
            P("tp"),
        ),
        out_specs=P("sp", "tp"),
        check_vma=False,
    )
```

time: 125 us -> 118 us (0.944)
  Pallas kernels: 0 us -> 27.4 us
  matrix products: 23 us -> 4.99 us
  other arithmetic: 22 us -> 9.65 us
  local copies, waits for them, and re-layouts: 11.2 us -> 5.08 us
  starting transfers between devices: 48 us -> 43 us
  waiting for transfers between devices: 5.24 us -> 9.2 us
  blocking collectives: 14.5 us -> 17.6 us
    pallas_call x0 -> x2, Pallas kernels: none -> 27.4 us  [the longest x1 18.8 us: on_device(): pl.pallas_call(functools.partial(window_kernel, tokens=tokens_here, seq_t...]
    dot_general x10 -> x0, matrix products: 17.9 us -> none  [the longest x2 4.96 us: attend_block(): jnp.einsum('qgrd,kgd->grqk', block_queries, block_keys, preferred_element...]
    unnamed x41 -> x15, local copies, waits for them, and re-layouts: 5.27 us -> 0.25 us
    reduce_sum x3 -> x1, other arithmetic: 5.2 us -> 1.04 us  [modulate(): spread = jnp.mean(jnp.square(values_f - center), -1, keepdims=True)]
    all_to_all x3, waiting for transfers between devices: 3.51 us -> 7.42 us  [copy_for_each(): return lax.all_to_all(copies, axis, split_axis=0, concat_axis=0, tiled=True)]
    and x2 -> x0, other arithmetic: 3.85 us -> none  [on_device(): (jnp.abs(query_pos[:, None] - key_pos[None, :]) <= WINDOW) & (key_pos >=...]
    rsqrt x3 -> x1, other arithmetic: 3.13 us -> 0.01 us  [modulate(): normed = (values_f - center) * lax.rsqrt(spread + norm_eps)]
    all_to_all x1, blocking collectives: 14.5 us -> 17.6 us  [from_same_cores(): lax.all_to_all(copies, axis, split_axis=0, concat_axis=0, tiled=True, axi...]
  transfers between devices with their start and end apart: 6 -> 6, of which waited for: 2 -> 3; matrix products, arithmetic and copies ran while one was open for 29% -> 12% of each run, Pallas kernels for 0% -> 16%
where the time goes in v2:
time: 118 us; the launch traced here: 117 us
  starting transfers between devices  43 us (36%)
  Pallas kernels  27.4 us (23%)
  blocking collectives  17.6 us (15%)
  other arithmetic  9.65 us (8%)
  waiting for transfers between devices  9.2 us (8%)
  local copies, waits for them, and re-layouts  5.08 us (4%)
  matrix products  4.99 us (4%)
    all_to_all x3, starting transfers between devices, copy_for_each(): return lax.all_to_all(copies, axis, split_axis=0, concat_axis=0, tiled=True)  35 us
    pallas_call x1, Pallas kernels, on_device(): pl.pallas_call(functools.partial(window_kernel, tokens=tokens_here, seq_t...  18.8 us
    all_to_all x1, blocking collectives, from_same_cores(): lax.all_to_all(copies, axis, split_axis=0, concat_axis=0, tiled=True, axi...  17.6 us
    pallas_call x1, Pallas kernels, on_device(): pl.pallas_call(context_kernel, grid=(blocks,), in_specs=[pl.BlockSpec((1,...  8.59 us
    all_to_all x3, waiting for transfers between devices, copy_for_each(): return lax.all_to_all(copies, axis, split_axis=0, concat_axis=0, tiled=True)  7.42 us
    ppermute x1, starting transfers between devices, swapped_cores(): return lax.ppermute(block, axis, [(i, i ^ 1) for i in range(count)])  3.79 us
    ppermute x1, starting transfers between devices, neighbour_rows(): low = lax.ppermute(rows[rows.shape[0] - width:], axis, forward)  2.95 us
  transfers between devices with their start and end apart: 6, of which 3 were waited for; matrix products, arithmetic and copies ran while one was open for 12% of the time, Pallas kernels for 16%

profile of v2, /device:TPU:1, one launch (start us, length us, event | category | flops | bytes accessed | tf_op | source)
XLA Modules:
  0.0 117.1 jit_solution(3359372918308699339)
XLA Ops:
  0.0 1.0 fusion.36
  1.1 0.9 broadcast_in_dim.10
  1.9 17.1 %all-to-all-start = ((f32[64,2,3,256]{3,1,2,0:T(2,128)}), f32[64,2,3,256]{3,1,2,0:T(2,128)S(1)}, u32[]{:S(2)}, u32[]{:S(2)}) async-start(f32[64,2,3,256]{3,1,2,0:T(2,128)} %broadcast_in_dim.10), calls=%async_computation | async-start | bytes 786432 | tf_op jit(solution)/shard_map/all_to_all | solution.py:24
  19.0 1.3 %fusion.45 = (bf16[128,2048]{1,0:T(8,128)(2,1)S(1)}, bf16[128,2048]{1,0:T(8,128)(2,1)S(1)}) fusion(bf16[1024,2048]{1,0:T(8,128)(2,1)} %latent_ref.1), kind=kLoop, calls=%fused_computation.71 | loop fusion | bytes 2097152 | tf_op jit(solution)/shard_map/slice | solution.py:46
  20.3 2.9 %collective-permute-start = (bf16[128,2048]{1,0:T(8,128)(2,1)S(1)}, bf16[128,2048]{1,0:T(8,128)(2,1)S(1)}, u32[]{:S(2)}, u32[]{:S(2)}) collective-permute-start(bf16[128,2048]{1,0:T(8,128)(2,1)S(1)} %get-tuple-element.11), channel_id=1, source_target_pairs={{0,8},{8,16},{16,24},{24,32},{32,40},{40,48},{48,56},{56,64},{64,7... | collective-permute-start | bytes 1572872 | tf_op jit(solution)/shard_map/ppermute | solution.py:46
  23.3 1.3 %collective-permute-start.1 = (bf16[128,2048]{1,0:T(8,128)(2,1)S(1)}, bf16[128,2048]{1,0:T(8,128)(2,1)}, u32[]{:S(2)}, u32[]{:S(2)}) collective-permute-start(bf16[128,2048]{1,0:T(8,128)(2,1)S(1)} %get-tuple-element.12), channel_id=1, source_target_pairs={{8,0},{16,8},{24,16},{32,24},{40,32},{48,40},{56,48},{64,56},{72,6... | collective-permute-start | bytes 1572872 | tf_op jit(solution)/shard_map/ppermute | solution.py:47
  25.4 1.0 convert_reduce_fusion
  26.4 0.7 broadcast_multiply_fusion.1
  27.1 1.0 fusion.13
  28.1 1.3 %sine_bitcast_fusion = (f32[32,1280]{1,0:T(8,128)}, f32[32,1280]{1,0:T(8,128)}) fusion(f32[1280,16]{0,1:T(8,128)S(1)} %get-tuple-element.21, f32[1280,16]{0,1:T(8,128)S(1)} %get-tuple-element.20), kind=kLoop, calls=%fused_computation.19 | loop fusion | flops 40960 | bytes 491520 | tf_op jit(solution)/shard_map/transpose | solution.py:328
  29.5 2.1 %pad_maximum_fusion.1.weight_ref = bf16[256,2048]{1,0:T(8,128)(2,1)} fusion(bf16[64,2048]{1,0:T(8,128)(2,1)} %bitcast.58, bf16[64,2048]{1,0:T(8,128)(2,1)} %bitcast.59, bf16[128,2048]{1,0:T(8,128)(2,1)S(1)} %bitcast.54), kind=kLoop, calls=%fused_computation.8 | loop fusion | flops 3145728 | bytes 2097152 | tf_op jit(solution)/shard_map/concatenate | solution.py:285
  31.6 2.6 %all-to-all-done = f32[64,2,3,256]{3,1,2,0:T(2,128)S(1)} async-done(((f32[64,2,3,256]{3,1,2,0:T(2,128)}), f32[64,2,3,256]{3,1,2,0:T(2,128)S(1)}, u32[]{:S(2)}, u32[]{:S(2)}) %all-to-all-start) | async-done | bytes 393248 | tf_op jit(solution)/shard_map/all_to_all | solution.py:24
  35.0 8.0 %all-to-all-start.1 = ((f32[8,2,3,256]{3,1,2,0:T(2,128)}), f32[8,2,3,256]{3,1,2,0:T(2,128)S(1)}, u32[]{:S(2)}, u32[]{:S(2)}) async-start(f32[8,2,3,256]{3,1,2,0:T(2,128)} %broadcast_in_dim.11), calls=%async_computation.1 | async-start | bytes 98304 | tf_op jit(solution)/shard_map/all_to_all | solution.py:24
  43.0 4.8 %all-to-all-done.1 = f32[8,2,3,256]{3,1,2,0:T(2,128)S(1)} async-done(((f32[8,2,3,256]{3,1,2,0:T(2,128)}), f32[8,2,3,256]{3,1,2,0:T(2,128)S(1)}, u32[]{:S(2)}, u32[]{:S(2)}) %all-to-all-start.1) | async-done | bytes 49184 | tf_op jit(solution)/shard_map/all_to_all | solution.py:24
  47.9 1.2 %convolution_convert_fusion = bf16[16,128]{1,0:T(8,128)(2,1)S(1)} fusion(bf16[2048,64]{0,1:T(8,128)(2,1)S(1)} %copy-done.4, bf16[2048,64]{0,1:T(8,128)(2,1)} %param.17, bf16[16,2048]{1,0:T(8,128)(2,1)S(1)} %copy-done.3, f32[2048]{0:T(1024)S(1)} %bitcast.62, f32[2048]{0:T(1024)S(1)} %bitcast.61, f32[16]{0:T(128)S(1)} %add_rsqrt_fusion, ...), kind=kOutput, calls=%fused_computation.6 | convolution fusion | flops 9635840 | bytes 610432 | tf_op jit(solution)/shard_map/dot_general | solution.py:277
  49.1 0.8 broadcast_in_dim.12
  49.9 9.8 %all-to-all-start.2 = ((bf16[64,16,128]{2,1,0:T(8,128)(2,1)}), bf16[64,16,128]{2,1,0:T(8,128)(2,1)S(1)}, u32[]{:S(2)}, u32[]{:S(2)}) async-start(bf16[64,16,128]{2,1,0:T(8,128)(2,1)} %broadcast_in_dim.12), calls=%async_computation.2 | async-start | bytes 524288 | tf_op jit(solution)/shard_map/all_to_all | solution.py:24
  59.7 2.1 %pad_maximum_fusion.halo_ref = bf16[256,2048]{1,0:T(8,128)(2,1)} fusion(bf16[128,2048]{1,0:T(8,128)(2,1)} %collective-permute-done.1, bf16[128,2048]{1,0:T(8,128)(2,1)S(1)} %collective-permute-done), kind=kLoop, calls=%fused_computation.7 | loop fusion | flops 2097152 | bytes 2097152 | tf_op jit(solution)/shard_map/concatenate | solution.py:48
  62.5 18.8 %window_part.1 = (bf16[8,64,256]{2,1,0:T(8,128)(2,1)}, f32[8,64,256]{2,1,0:T(8,128)}, f32[8,8,256]{2,1,0:T(8,128)}) custom-call(s32[1]{0:T(128)} %bitcast.5.start_ref, bf16[1024,2048]{1,0:T(8,128)(2,1)} %latent_ref.1, bf16[256,2048]{1,0:T(8,128)(2,1)} %pad_maximum_fusion.halo_ref, bf16[256,2048]{1,0:T(8,128)(2,1)} %pad_maximum_fusion.1.weight_ref, ...), custom_call_target="tpu_custom_call" | custom-call | tf_op jit(solution)/shard_map/window_part/pallas_call | solution.py:291
  82.6 8.6 %context_part.1 = bf16[4,1024,128]{2,1,0:T(8,128)(2,1)} custom-call(bf16[8,64,256]{2,1,0:T(8,128)(2,1)} %get-tuple-element.8.queries_ref, f32[8,64,256]{2,1,0:T(8,128)} %get-tuple-element.9.partial_ref, f32[8,8,256]{2,1,0:T(8,128)} %get-tuple-element.10.stats_ref, bf16[1024,128]{1,0:T(8,128)(2,1)} %bitcast.55, f32[1,256]{1,0:T(1,128)} %bitcast.64, ...), custom_call_target="tpu_custom_call" | custom-call | tf_op jit(solution)/shard_map/context_part/pallas_call | solution.py:331
  91.2 17.6 %all_to_all.20 = bf16[4,1024,128]{2,1,0:T(8,128)(2,1)S(1)} all-to-all(bf16[4,1024,128]{2,1,0:T(8,128)(2,1)} %context_part.1), channel_id=1, replica_groups={{0,2,4,6},{1,3,5,7},{8,10,12,14},{9,11,13,15},{16,18,20,22},{17,19,21,2..., dimensions={0} | all-to-all | bytes 2097152 | tf_op jit(solution)/shard_map/all_to_all | solution.py:54
  108.8 3.8 %collective-permute-start.2 = (bf16[4,1024,128]{2,1,0:T(8,128)(2,1)S(1)}, bf16[4,1024,128]{2,1,0:T(8,128)(2,1)S(1)}, u32[]{:S(2)}, u32[]{:S(2)}) collective-permute-start(bf16[4,1024,128]{2,1,0:T(8,128)(2,1)S(1)} %all_to_all.20), channel_id=1, source_target_pairs={{0,1},{1,0},{2,3},{3,2},{4,5},{5,4},{6,7},{7,6},{8,9},{9,8},{10,11... | collective-permute-start | bytes 3145736 | tf_op jit(solution)/shard_map/ppermute | solution.py:61
  113.1 1.8 %collective-permute-done.2 = bf16[4,1024,128]{2,1,0:T(8,128)(2,1)S(1)} collective-permute-done((bf16[4,1024,128]{2,1,0:T(8,128)(2,1)S(1)}, bf16[4,1024,128]{2,1,0:T(8,128)(2,1)S(1)}, u32[]{:S(2)}, u32[]{:S(2)}) %collective-permute-start.2) | collective-permute-done | bytes 1048608 | tf_op jit(solution)/shard_map/ppermute | solution.py:61
  114.9 2.3 %fusion.3 = bf16[1024,256]{1,0:T(8,128)(2,1)} fusion(f32[1024,256]{1,0:T(8,128)S(1)} %convolution_bitcast_fusion.1, bf16[4,1024,128]{2,1,0:T(8,128)(2,1)S(1)} %collective-permute-done.2, f32[256]{0:T(256)S(1)} %bitcast.63, bf16[1024,2048]{1,0:T(8,128)(2,1)} %latent_ref.1, s32[]{:T(128)S(6)} %select_n.37, bf16[4,2,128,256]{3,2,1,0:T(8,128)(2,1)S(1)} %bitcast.52, ...), kind=kOutput, calls=%fused_computation.5 | convolution fusion | flops 269746176 | bytes 3408904 | tf_op jit(solution)/shard_map/xrk,xkn->rn/dot_general | solution.py:362
  (31 shorter events, 4.0 us)
Async XLA Ops:
  0.0 112.6 %copy-start = (bf16[1024,256]{1,0:T(8,128)(2,1)S(1)}, bf16[1024,256]{1,0:T(8,128)(2,1)}, u32[]{:S(2)}) copy-start(bf16[1024,256]{1,0:T(8,128)(2,1)} %param.19) | copy-start | bytes 1572868
  0.0 25.1 %copy-start.2 = (bf16[2048,128]{1,0:T(8,128)(2,1)S(1)}, bf16[2048,128]{1,0:T(8,128)(2,1)}, u32[]{:S(2)}) copy-start(bf16[2048,128]{1,0:T(8,128)(2,1)} %param.16) | copy-start | bytes 1572868
  1.9 32.3 %all-to-all-start = ((f32[64,2,3,256]{3,1,2,0:T(2,128)}), f32[64,2,3,256]{3,1,2,0:T(2,128)S(1)}, u32[]{:S(2)}, u32[]{:S(2)}) async-start(f32[64,2,3,256]{3,1,2,0:T(2,128)} %broadcast_in_dim.10), calls=%async_computation | async-start | bytes 786432 | tf_op jit(solution)/shard_map/all_to_all | solution.py:24
  20.3 39.4 %collective-permute-start = (bf16[128,2048]{1,0:T(8,128)(2,1)S(1)}, bf16[128,2048]{1,0:T(8,128)(2,1)S(1)}, u32[]{:S(2)}, u32[]{:S(2)}) collective-permute-start(bf16[128,2048]{1,0:T(8,128)(2,1)S(1)} %get-tuple-element.11), channel_id=1, source_target_pairs={{0,8},{8,16},{16,24},{24,32},{32,40},{40,48},{48,56},{56,64},{64,7... | collective-permute-start | bytes 1572872 | tf_op jit(solution)/shard_map/ppermute | solution.py:46
  23.3 36.4 %collective-permute-start.1 = (bf16[128,2048]{1,0:T(8,128)(2,1)S(1)}, bf16[128,2048]{1,0:T(8,128)(2,1)}, u32[]{:S(2)}, u32[]{:S(2)}) collective-permute-start(bf16[128,2048]{1,0:T(8,128)(2,1)S(1)} %get-tuple-element.12), channel_id=1, source_target_pairs={{8,0},{16,8},{24,16},{32,24},{40,32},{48,40},{56,48},{64,56},{72,6... | collective-permute-start | bytes 1572872 | tf_op jit(solution)/shard_map/ppermute | solution.py:47
  25.4 22.5 %copy-start.3 = (bf16[16,2048]{1,0:T(8,128)(2,1)S(1)}, bf16[16,2048]{1,0:T(8,128)(2,1)}, u32[]{:S(2)}) copy-start(bf16[16,2048]{1,0:T(8,128)(2,1)} %param.12) | copy-start | bytes 196612
  25.4 22.5 %copy-start.4 = (bf16[2048,64]{0,1:T(8,128)(2,1)S(1)}, bf16[2048,64]{0,1:T(8,128)(2,1)}, u32[]{:S(2)}) copy-start(bf16[2048,64]{0,1:T(8,128)(2,1)} %param.18) | copy-start | bytes 786436
  35.0 12.8 %all-to-all-start.1 = ((f32[8,2,3,256]{3,1,2,0:T(2,128)}), f32[8,2,3,256]{3,1,2,0:T(2,128)S(1)}, u32[]{:S(2)}, u32[]{:S(2)}) async-start(f32[8,2,3,256]{3,1,2,0:T(2,128)} %broadcast_in_dim.11), calls=%async_computation.1 | async-start | bytes 98304 | tf_op jit(solution)/shard_map/all_to_all | solution.py:24
  49.9 31.4 %all-to-all-start.2 = ((bf16[64,16,128]{2,1,0:T(8,128)(2,1)}), bf16[64,16,128]{2,1,0:T(8,128)(2,1)S(1)}, u32[]{:S(2)}, u32[]{:S(2)}) async-start(bf16[64,16,128]{2,1,0:T(8,128)(2,1)} %broadcast_in_dim.12), calls=%async_computation.2 | async-start | bytes 524288 | tf_op jit(solution)/shard_map/all_to_all | solution.py:24
  62.5 18.8 %copy-start.5 = (f32[2]{0:T(128)S(1)}, f32[2]{0:T(128)}, u32[]{:S(2)}) copy-start(f32[2]{0:T(128)} %param.20) | copy-start | bytes 28
  62.5 19.5 %copy-start.6 = (f32[2]{0:T(128)S(1)}, f32[2]{0:T(128)}, u32[]{:S(2)}) copy-start(f32[2]{0:T(128)} %param.21) | copy-start | bytes 28
  81.2 1.3 %copy-start.1 = (bf16[64,16,128]{2,1,0:T(8,128)(2,1)}, bf16[64,16,128]{2,1,0:T(8,128)(2,1)S(1)}, u32[]{:S(2)}) copy-start(bf16[64,16,128]{2,1,0:T(8,128)(2,1)S(1)} %all-to-all-done.2) | copy-start | bytes 786436
  108.8 6.1 %collective-permute-start.2 = (bf16[4,1024,128]{2,1,0:T(8,128)(2,1)S(1)}, bf16[4,1024,128]{2,1,0:T(8,128)(2,1)S(1)}, u32[]{:S(2)}, u32[]{:S(2)}) collective-permute-start(bf16[4,1024,128]{2,1,0:T(8,128)(2,1)S(1)} %all_to_all.20), channel_id=1, source_target_pairs={{0,1},{1,0},{2,3},{3,2},{4,5},{5,4},{6,7},{7,6},{8,9},{9,8},{10,11... | collective-permute-start | bytes 3145736 | tf_op jit(solution)/shard_map/ppermute | solution.py:61
